TPU v7x, 128 devices: a whole 4x4x4 slice. The times are simulated.
128 devices in a mesh: ra: 16 (over z, x), cb: 4 (over y), dp: 2 (over core).
Axes of the slice: x: 4, y: 4, z: 4, core: 2. Of those that a mesh axis runs over, the one named last changes fastest.
Arguments:
- carried: bfloat16 [3072, 4096], P('dp', 'ra'), may hold values from -100 to 100
- branch_in: bfloat16 [3072, 4096], P('dp', 'ra'), may hold values from -12 to 12
- gain_in: float32 [4096], P('ra'), may hold values from 0.1 to 1.9
- bias_in: float32 [4096], P('ra'), may hold values from -1.8 to 1.8
- up_weight: bfloat16 [4096, 16384], P('ra', 'cb'), may hold values from -0.125 to 0.125
- down_weight: bfloat16 [16384, 4096], P('cb', 'ra'), may hold values from -0.046875 to 0.046875
- gain_out: float32 [4096], P('ra'), may hold values from 0.1 to 1.9
- bias_out: float32 [4096], P('ra'), may hold values from -1.8 to 1.8
Outputs:
- layer_out: bfloat16 [3072, 4096], P('dp', 'ra')
All inputs are finite; a program needn't handle non-finite values.
Results may differ from a plain program's by a relative error of at most 0.006.
Values may be sent and summed in bfloat16 or wider, within the bound.
A program may use at most 64 MiB of HBM per device.

v0:
```python
import jax
import jax.numpy as jnp
from jax import lax
from jax.sharding import PartitionSpec as P

residual_scale = 2.0**0.25
norm_eps = 1e-05


def copy_for_each(array, axis):
    length = lax.axis_size(axis)
    return lax.all_to_all(
        jnp.broadcast_to(array[None], (length, *array.shape)), axis, 0, 0, tiled=True
    )


def of_everyone(array, axis):
    return copy_for_each(array, axis).sum(axis=0)


def packed_total(arrays, axis):
    ravelled, at, done = (jnp.concatenate([a.reshape(-1) for a in arrays]), 0, [])
    running = of_everyone(ravelled, axis)
    for a in arrays:
        done.append(running[at : at + a.size].reshape(a.shape))
        at += a.size
    return tuple(done)


def taken_together(array, axis):
    return copy_for_each(array, axis).astype(jnp.float32).sum(axis=0)


def normalize(mixed, totals, squares, width, gain, bias):
    mean = totals[:, None] / width
    spread = squares[:, None] / width - mean * mean
    return (mixed - mean) * lax.rsqrt(spread + norm_eps) * gain + bias


def per_device(carried, branch_in, gain_in, bias_in, up_weight, down_weight, gain_out, bias_out):
    width = carried.shape[1] * lax.axis_size("ra")
    mixed_in = residual_scale * carried.astype(jnp.float32) + branch_in.astype(jnp.float32)
    totals, squares = packed_total(
        (jnp.sum(mixed_in, axis=1), jnp.sum(mixed_in * mixed_in, axis=1)), "ra"
    )
    normed = normalize(mixed_in, totals, squares, width, gain_in, bias_in).astype(jnp.bfloat16)
    regrouped = lax.all_to_all(up_weight, "ra", split_axis=1, concat_axis=0, tiled=True)
    pre_share = lax.dot_general(
        regrouped,
        lax.all_gather(normed, "ra", axis=1, tiled=True),
        (((0,), (1,)), ((), ())),
        preferred_element_type=jnp.float32,
    )
    hidden_share = jnp.square(jnp.maximum(pre_share, 0.0)).astype(jnp.bfloat16)
    branch_part = lax.dot_general(
        lax.all_gather(hidden_share, "ra", axis=0, tiled=True),
        down_weight,
        (((0,), (0,)), ((), ())),
        preferred_element_type=jnp.float32,
    )
    branch_out = taken_together(branch_part.astype(jnp.bfloat16), "cb").astype(jnp.float32)
    mixed_out = residual_scale * normed.astype(jnp.float32) + branch_out
    totals_out, squares_out = packed_total(
        (jnp.sum(mixed_out, axis=1), jnp.sum(mixed_out * mixed_out, axis=1)), "ra"
    )
    return normalize(mixed_out, totals_out, squares_out, width, gain_out, bias_out).astype(
        jnp.bfloat16
    )


def solution(mesh):
    in_specs = (
        P("dp", "ra"),
        P("dp", "ra"),
        P("ra"),
        P("ra"),
        P("ra", "cb"),
        P("cb", "ra"),
        P("ra"),
        P("ra"),
    )
    out_specs = P("dp", "ra")
    return jax.shard_map(
        per_device, mesh=mesh, in_specs=in_specs, out_specs=out_specs, check_vma=False
    )
```

profile of v0, /device:TPU:0, one launch (start us, length us, event | category | flops | bytes accessed | tf_op | source)
XLA Modules:
  0.0 324.9 jit_solution(11136814874928397678)
XLA Ops:
  6.5 0.0 copy-start
  6.5 0.0 copy-start.3
  6.5 0.0 copy-start.4
  6.5 0.0 copy-start.5
  6.5 0.0 all-gather.3.cloned.1.call-start
  6.6 2.1 fusion.3
  8.7 0.1 broadcast_in_dim.6
  8.8 16.1 %all_to_all.36 = f32[16,1,3072]{2,1,0:T(1,128)S(1)} all-to-all(f32[16,1,3072]{2,1,0:T(1,128)S(1)} %broadcast_in_dim.6), channel_id=1, replica_groups=mesh['ra'=16,'cb'=4,'dp'=2] {'ra'}, dimensions={0} | all-to-all | bytes 393216 | tf_op jit(solution)/shard_map/all_to_all | solution.py:12
  24.9 0.1 reduce_sum.65
  25.1 0.0 copy-done.3
  25.1 0.0 copy-done.4
  25.1 0.0 copy-done.5
  25.1 2.5 add_convert_fusion.1
  27.6 0.0 all-gather.3.cloned.1.call-update
  27.6 0.0 all-gather.5.cloned.1.call-start
  27.7 4.1 %copy.14 = bf16[256,4096]{0,1:T(8,128)(2,1)} copy(bf16[256,4096]{1,0:T(8,128)(2,1)} %param.12) | data formatting | bytes 4194304 | tf_op args[4]
  31.7 44.3 %all_to_all.37 = bf16[256,16,256]{0,2,1:T(8,128)(2,1)} all-to-all(bf16[256,16,256]{0,2,1:T(8,128)(2,1)} %bitcast.10), channel_id=1, replica_groups=mesh['ra'=16,'cb'=4,'dp'=2] {'ra'}, dimensions={1} | all-to-all | bytes 4194304 | tf_op jit(solution)/shard_map/all_to_all | solution.py:47
  76.0 3.9 %copy.15 = bf16[16,256,256]{2,1,0:T(8,128)(2,1)} copy(bf16[16,256,256]{1,2,0:T(8,128)(2,1)} %bitcast.9) | data formatting | bytes 4194304 | tf_op jit(solution)/shard_map/all_to_all | solution.py:47
  79.9 65.2 %all-gather.3.cloned.1.call-done = bf16[1536,4096]{1,0:T(8,128)(2,1)} async-done(((bf16[1536,256]{1,0:T(8,128)(2,1)}), bf16[1536,4096]{1,0:T(8,128)(2,1)}) %all-gather.3.cloned.1.call-update) | async-done | bytes 12582928 | tf_op jit(solution)/shard_map/all_gather | solution.py:50
  145.1 9.6 %fusion.2 = bf16[256,1536]{0,1:T(8,128)(2,1)} fusion(bf16[1536,4096]{1,0:T(8,128)(2,1)} %all-gather.3.cloned.1.call-done, bf16[4096,256]{1,0:T(8,128)(2,1)} %bitcast.11), kind=kOutput, calls=%fused_computation.5 | convolution fusion | flops 3222405120 | bytes 15466496 | tf_op jit(solution)/shard_map/dot_general | solution.py:48
  154.7 0.0 all-gather.5.cloned.1.call-update
  154.7 98.0 %all-gather.5.cloned.1.call-done = bf16[4096,1536]{0,1:T(8,128)(2,1)} async-done(((bf16[256,1536]{0,1:T(8,128)(2,1)}), bf16[4096,1536]{0,1:T(8,128)(2,1)}) %all-gather.5.cloned.1.call-update) | async-done | bytes 12582928 | tf_op jit(solution)/shard_map/all_gather | solution.py:56
  252.8 0.0 copy-done
  252.8 6.5 %convolution_convert_fusion = bf16[1536,256]{1,0:T(8,128)(2,1)S(1)} fusion(bf16[4096,1536]{0,1:T(8,128)(2,1)} %all-gather.5.cloned.1.call-done, bf16[4096,256]{1,0:T(8,128)(2,1)S(1)} %copy-done), kind=kOutput, calls=%fused_computation.4 | convolution fusion | flops 3221618688 | bytes 15466496 | tf_op jit(solution)/shard_map/dot_general | solution.py:55
  259.3 0.2 broadcast_in_dim.7
  259.5 40.3 %all_to_all.38 = bf16[4,1536,256]{2,1,0:T(8,128)(2,1)S(1)} all-to-all(bf16[4,1536,256]{2,1,0:T(8,128)(2,1)S(1)} %broadcast_in_dim.7), channel_id=1, replica_groups=mesh['ra'=16,'cb'=4,'dp'=2] {'cb'}, dimensions={0} | all-to-all | bytes 6291456 | tf_op jit(solution)/shard_map/all_to_all | solution.py:12
  299.8 0.0 copy-start.2
  299.8 0.5 convert_reduce_fusion
  300.2 0.0 copy-start.1
  300.2 1.1 copy-done.1
  301.4 0.0 copy-done.2
  301.4 0.0 copy-start.6
  301.4 0.0 copy-start.7
  301.4 0.5 fusion.4
  301.9 0.1 broadcast_in_dim.8
  302.0 13.1 %all_to_all.39 = f32[16,1,3072]{2,1,0:T(1,128)S(1)} all-to-all(f32[16,1,3072]{2,1,0:T(1,128)S(1)} %broadcast_in_dim.8), channel_id=1, replica_groups=mesh['ra'=16,'cb'=4,'dp'=2] {'ra'}, dimensions={0} | all-to-all | bytes 393216 | tf_op jit(solution)/shard_map/all_to_all | solution.py:12
  315.1 0.1 reduce_sum.69
  315.3 0.0 copy-done.6
  315.3 0.0 copy-done.7
  315.3 2.8 add_convert_fusion
  (4 shorter events, 0.0 us)
Async XLA Ops:
  6.5 246.2 %copy-start = (bf16[4096,256]{1,0:T(8,128)(2,1)S(1)}, bf16[4096,256]{1,0:T(8,128)(2,1)}, u32[]{:S(2)}) copy-start(bf16[4096,256]{1,0:T(8,128)(2,1)} %param.13) | copy-start | bytes 6291460
  6.5 18.5 %copy-start.3 = (bf16[1536,256]{1,0:T(8,128)(2,1)S(1)}, bf16[1536,256]{1,0:T(8,128)(2,1)}, u32[]{:S(2)}) copy-start(bf16[1536,256]{1,0:T(8,128)(2,1)} %param.9) | copy-start | bytes 2359300
  6.5 18.5 %copy-start.4 = (f32[256]{0:T(256)S(1)}, f32[256]{0:T(256)}, u32[]{:S(2)}) copy-start(f32[256]{0:T(256)} %param.11) | copy-start | bytes 3076
  6.5 18.5 %copy-start.5 = (f32[256]{0:T(256)S(1)}, f32[256]{0:T(256)}, u32[]{:S(2)}) copy-start(f32[256]{0:T(256)} %param.10) | copy-start | bytes 3076
  6.5 138.6 %all-gather.3.cloned.1.call-start = ((), (), s32[]{:S(2)}) async-start(), calls=%async_computation.4 | async-start | bytes 13369344 | tf_op jit(solution)/shard_map/all_gather | solution.py:50
  27.6 225.1 %all-gather.5.cloned.1.call-start = ((), (), s32[]{:S(2)}) async-start(), calls=%async_computation.5 | async-start | bytes 13369344 | tf_op jit(solution)/shard_map/all_gather | solution.py:56
  299.8 1.6 copy-start.2
  300.2 1.2 copy-start.1
  301.4 13.9 %copy-start.6 = (f32[256]{0:T(256)S(1)}, f32[256]{0:T(256)}, u32[]{:S(2)}) copy-start(f32[256]{0:T(256)} %param.15) | copy-start | bytes 3076
  301.4 13.9 %copy-start.7 = (f32[256]{0:T(256)S(1)}, f32[256]{0:T(256)}, u32[]{:S(2)}) copy-start(f32[256]{0:T(256)} %param.14) | copy-start | bytes 3076
Sparse Core Ops, SparseCore 0:
  27.7 117.3 all-gather.2
  154.9 97.8 all-gather.4
where the time goes:
time: 325 us
  waiting for transfers between devices  163 us (50%)
  blocking collectives  114 us (35%)
  matrix products  16.1 us (5%)
  between operations  13.5 us (4%)
  local copies, waits for them, and re-layouts  9.57 us (3%)
  other arithmetic  8.59 us (3%)
    all_gather x1, waiting for transfers between devices, per_device(): lax.all_gather(hidden_share, 'ra', axis=0, tiled=True)  98 us
    all_to_all x3, blocking collectives, copy_for_each(): lax.all_to_all(jnp.broadcast_to(array[None], (length, *array.shape)), axi...  69.5 us
    all_gather x1, waiting for transfers between devices, per_device(): lax.all_gather(normed, 'ra', axis=1, tiled=True)  65.2 us
    all_to_all x1, blocking collectives, per_device(): lax.all_to_all(up_weight, 'ra', split_axis=1, concat_axis=0, tiled=True)  44.3 us
    dot_general x1, matrix products, per_device(): lax.dot_general(regrouped, lax.all_gather(normed, 'ra', axis=1, tiled=Tru...  9.57 us
  transfers between devices with their start and end apart: 2, of which 2 were waited for; matrix products, arithmetic and copies ran while one was open for 2% of the time, Pallas kernels for 0%

commit v1 on v0

--- a/solution.py
+++ b/solution.py
@@ -5,6 +5,18 @@
 
 residual_scale = 2.0**0.25
 norm_eps = 1e-05
+
+
+def gather_by_bits(shard, axis, dim):
+    ways, here = (lax.axis_size(axis), lax.axis_index(axis))
+    grown, reach = (shard, 1)
+    while reach < ways:
+        theirs = lax.ppermute(grown, axis, [(d, d ^ reach) for d in range(ways)])
+        mine_first = jnp.concatenate([grown, theirs], axis=dim)
+        theirs_first = jnp.concatenate([theirs, grown], axis=dim)
+        grown = jnp.where(here & reach == 0, mine_first, theirs_first)
+        reach = 2 * reach
+    return grown
 
 
 def copy_for_each(array, axis):
@@ -47,7 +59,7 @@
     regrouped = lax.all_to_all(up_weight, "ra", split_axis=1, concat_axis=0, tiled=True)
     pre_share = lax.dot_general(
         regrouped,
-        lax.all_gather(normed, "ra", axis=1, tiled=True),
+        gather_by_bits(normed, "ra", 1),
         (((0,), (1,)), ((), ())),
         preferred_element_type=jnp.float32,
     )

time: 325 us -> 510 us (1.57)
  waiting for transfers between devices: 163 us -> 363 us
  blocking collectives: 114 us -> 69.5 us
  other arithmetic: 8.59 us -> 26.3 us
  starting transfers between devices: 0.08 us -> 8.53 us
    all_to_all x0 -> x1, waiting for transfers between devices: none -> 147 us  [per_device(): lax.all_to_all(up_weight, 'ra', split_axis=1, concat_axis=0, tiled=True)]
    ppermute x0 -> x4, waiting for transfers between devices: none -> 119 us  [gather_by_bits(): theirs = lax.ppermute(grown, axis, [(d, d ^ reach) for d in range(ways)])]
    all_gather x1 -> x0, waiting for transfers between devices: 65.2 us -> none  [per_device(): lax.all_gather(normed, 'ra', axis=1, tiled=True)]
    all_to_all x1 -> x0, blocking collectives: 44.3 us -> none  [per_device(): lax.all_to_all(up_weight, 'ra', split_axis=1, concat_axis=0, tiled=True)]
    select_n x0 -> x3, other arithmetic: none -> 18.4 us  [gather_by_bits(): grown = jnp.where(here & reach == 0, mine_first, theirs_first)]
  transfers between devices with their start and end apart: 2 -> 6, of which waited for: 2 -> 5; matrix products, arithmetic and copies ran while one was open for 2% -> 2% of each run, Pallas kernels for 0% -> 0%
where the time goes in v1:
time: 510 us
  waiting for transfers between devices  363 us (71%)
  blocking collectives  69.5 us (14%)
  other arithmetic  26.3 us (5%)
  matrix products  19 us (4%)
  between operations  13.6 us (3%)
  local copies, waits for them, and re-layouts  9.55 us (2%)
  starting transfers between devices  8.53 us (2%)
    all_to_all x1, waiting for transfers between devices, per_device(): lax.all_to_all(up_weight, 'ra', split_axis=1, concat_axis=0, tiled=True)  147 us
    ppermute x4, waiting for transfers between devices, gather_by_bits(): theirs = lax.ppermute(grown, axis, [(d, d ^ reach) for d in range(ways)])  119 us
    all_gather x1, waiting for transfers between devices, per_device(): lax.all_gather(hidden_share, 'ra', axis=0, tiled=True)  97.6 us
    all_to_all x3, blocking collectives, copy_for_each(): lax.all_to_all(jnp.broadcast_to(array[None], (length, *array.shape)), axi...  69.5 us
    select_n x3, other arithmetic, gather_by_bits(): grown = jnp.where(here & reach == 0, mine_first, theirs_first)  18.4 us
    dot_general x1, matrix products, per_device(): lax.dot_general(regrouped, gather_by_bits(normed, 'ra', 1), (((0,), (1,))...  12.5 us
  transfers between devices with their start and end apart: 6, of which 5 were waited for; matrix products, arithmetic and copies ran while one was open for 2% of the time, Pallas kernels for 0%

profile of v1, /device:TPU:0, one launch (start us, length us, event | category | flops | bytes accessed | tf_op | source)
XLA Modules:
  0.0 510.0 jit_solution(7866510448810644576)
XLA Ops:
  6.5 0.0 copy-start
  6.5 0.0 copy-start.2
  6.5 0.0 copy-start.3
  6.5 2.1 fusion.11
  8.6 0.1 broadcast_in_dim.6
  8.7 16.1 %all_to_all.36 = f32[16,1,3072]{2,1,0:T(1,128)S(1)} all-to-all(f32[16,1,3072]{2,1,0:T(1,128)S(1)} %broadcast_in_dim.6), channel_id=1, replica_groups=mesh['ra'=16,'cb'=4,'dp'=2] {'ra'}, dimensions={0} | all-to-all | bytes 393216 | tf_op jit(solution)/shard_map/all_to_all | solution.py:24
  24.9 0.1 reduce_sum.65
  25.0 0.0 copy-done.2
  25.0 0.0 copy-done.3
  25.0 1.8 add_convert_fusion.1
  26.9 0.6 collective-permute-start
  27.5 17.4 %collective-permute-done = bf16[1536,256]{1,0:T(8,128)(2,1)} collective-permute-done((bf16[1536,256]{1,0:T(8,128)(2,1)S(1)}, bf16[1536,256]{1,0:T(8,128)(2,1)}, u32[]{:S(2)}, u32[]{:S(2)}) %collective-permute-start) | collective-permute-done | bytes 786464 | tf_op jit(solution)/shard_map/ppermute | solution.py:14
  44.9 2.9 maximum_select_fusion.12
  47.8 1.4 collective-permute-start.1
  49.2 34.3 %collective-permute-done.1 = bf16[1536,512]{1,0:T(8,128)(2,1)} collective-permute-done((bf16[1536,512]{1,0:T(8,128)(2,1)}, bf16[1536,512]{1,0:T(8,128)(2,1)}, u32[]{:S(2)}, u32[]{:S(2)}) %collective-permute-start.1) | collective-permute-done | bytes 1572896 | tf_op jit(solution)/shard_map/ppermute | solution.py:14
  83.5 5.3 %maximum_select_fusion.3 = bf16[1536,1024]{1,0:T(8,128)(2,1)} fusion(bf16[1536,512]{1,0:T(8,128)(2,1)} %collective-permute-done.1, bf16[1536,512]{1,0:T(8,128)(2,1)} %maximum_select_fusion.12, pred[]{:T(512)S(6)} %eq.14), kind=kLoop, calls=%fused_computation.10 | loop fusion | flops 14155776 | bytes 6291457 | tf_op jit(solution)/shard_map/jit(_where)/select_n | solution.py:17
  88.8 0.1 collective-permute-start.2
  88.9 66.9 %collective-permute-done.2 = bf16[1536,1024]{1,0:T(8,128)(2,1)} collective-permute-done((bf16[1536,1024]{1,0:T(8,128)(2,1)}, bf16[1536,1024]{1,0:T(8,128)(2,1)}, u32[]{:S(2)}, u32[]{:S(2)}) %collective-permute-start.2) | collective-permute-done | bytes 3145760 | tf_op jit(solution)/shard_map/ppermute | solution.py:14
  155.8 10.2 %maximum_select_fusion.2 = bf16[1536,2048]{1,0:T(8,128)(2,1)} fusion(bf16[1536,1024]{1,0:T(8,128)(2,1)} %collective-permute-done.2, bf16[1536,1024]{1,0:T(8,128)(2,1)} %maximum_select_fusion.3, pred[]{:T(512)S(6)} %eq.13), kind=kLoop, calls=%fused_computation.8 | loop fusion | flops 28311552 | bytes 12582913 | tf_op jit(solution)/shard_map/jit(_where)/select_n | solution.py:17
  166.0 1.8 collective-permute-start.3
  167.8 4.1 copy.14
  171.9 4.6 all-to-all-start.1
  176.4 0.0 all-gather.2.cloned.1.call-start
  176.5 147.3 %all-to-all-done.1 = bf16[256,16,256]{0,2,1:T(8,128)(2,1)} async-done(((bf16[256,16,256]{0,2,1:T(8,128)(2,1)}), bf16[256,16,256]{0,2,1:T(8,128)(2,1)}, u32[]{:S(2)}, u32[]{:S(2)}) %all-to-all-start.1) | async-done | bytes 2097184 | tf_op jit(solution)/shard_map/all_to_all | solution.py:59
  323.8 3.9 copy.15
  327.7 0.0 collective-permute-done.3
  327.7 12.5 %fusion.10 = bf16[256,1536]{0,1:T(8,128)(2,1)} fusion(bf16[4096,256]{1,0:T(8,128)(2,1)} %bitcast.9, bf16[1536,2048]{1,0:T(8,128)(2,1)} %collective-permute-done.3, bf16[1536,2048]{1,0:T(8,128)(2,1)} %maximum_select_fusion.2, pred[]{:T(512)S(6)} %eq.12), kind=kOutput, calls=%fused_computation.15 | convolution fusion | flops 3279028224 | bytes 15466497 | tf_op jit(solution)/shard_map/dot_general | solution.py:60
  340.2 0.0 all-gather.2.cloned.1.call-update
  340.3 97.6 %all-gather.2.cloned.1.call-done = bf16[4096,1536]{0,1:T(8,128)(2,1)} async-done(((bf16[256,1536]{0,1:T(8,128)(2,1)}), bf16[4096,1536]{0,1:T(8,128)(2,1)}) %all-gather.2.cloned.1.call-update) | async-done | bytes 12582928 | tf_op jit(solution)/shard_map/all_gather | solution.py:68
  437.8 0.0 copy-done
  437.8 6.5 %convolution_convert_fusion = bf16[1536,256]{1,0:T(8,128)(2,1)S(1)} fusion(bf16[4096,1536]{0,1:T(8,128)(2,1)} %all-gather.2.cloned.1.call-done, bf16[4096,256]{1,0:T(8,128)(2,1)S(1)} %copy-done), kind=kOutput, calls=%fused_computation.14 | convolution fusion | flops 3221618688 | bytes 15466496 | tf_op jit(solution)/shard_map/dot_general | solution.py:67
  444.3 0.2 broadcast_in_dim.7
  444.6 40.3 %all_to_all.37 = bf16[4,1536,256]{2,1,0:T(8,128)(2,1)S(1)} all-to-all(bf16[4,1536,256]{2,1,0:T(8,128)(2,1)S(1)} %broadcast_in_dim.7), channel_id=1, replica_groups=mesh['ra'=16,'cb'=4,'dp'=2] {'cb'}, dimensions={0} | all-to-all | bytes 6291456 | tf_op jit(solution)/shard_map/all_to_all | solution.py:24
  484.8 0.5 convert_reduce_fusion
  485.3 0.0 copy-start.1
  485.3 1.1 copy-done.1
  486.5 0.0 copy-start.4
  486.5 0.0 copy-start.5
  486.5 0.5 fusion.12
  487.0 0.1 broadcast_in_dim.8
  487.1 13.1 %all_to_all.38 = f32[16,1,3072]{2,1,0:T(1,128)S(1)} all-to-all(f32[16,1,3072]{2,1,0:T(1,128)S(1)} %broadcast_in_dim.8), channel_id=1, replica_groups=mesh['ra'=16,'cb'=4,'dp'=2] {'ra'}, dimensions={0} | all-to-all | bytes 393216 | tf_op jit(solution)/shard_map/all_to_all | solution.py:24
  500.2 0.1 reduce_sum.69
  500.4 0.0 copy-done.4
  500.4 0.0 copy-done.5
  500.4 2.8 add_convert_fusion
  (4 shorter events, 0.0 us)
Async XLA Ops:
  6.5 431.3 %copy-start = (bf16[4096,256]{1,0:T(8,128)(2,1)S(1)}, bf16[4096,256]{1,0:T(8,128)(2,1)}, u32[]{:S(2)}) copy-start(bf16[4096,256]{1,0:T(8,128)(2,1)} %param.13) | copy-start | bytes 6291460
  6.5 18.5 %copy-start.2 = (f32[256]{0:T(256)S(1)}, f32[256]{0:T(256)}, u32[]{:S(2)}) copy-start(f32[256]{0:T(256)} %param.11) | copy-start | bytes 3076
  6.5 18.5 %copy-start.3 = (f32[256]{0:T(256)S(1)}, f32[256]{0:T(256)}, u32[]{:S(2)}) copy-start(f32[256]{0:T(256)} %param.10) | copy-start | bytes 3076
  26.9 18.0 %collective-permute-start = (bf16[1536,256]{1,0:T(8,128)(2,1)S(1)}, bf16[1536,256]{1,0:T(8,128)(2,1)}, u32[]{:S(2)}, u32[]{:S(2)}) collective-permute-start(bf16[1536,256]{1,0:T(8,128)(2,1)S(1)} %add_convert_fusion.1), channel_id=1, source_target_pairs={{0,8},{8,0},{16,24},{24,16},{32,40},{40,32},{48,56},{56,48},{64,72... | collective-permute-start | bytes 2359304 | tf_op jit(solution)/shard_map/ppermute | solution.py:14
  47.8 35.7 %collective-permute-start.1 = (bf16[1536,512]{1,0:T(8,128)(2,1)}, bf16[1536,512]{1,0:T(8,128)(2,1)}, u32[]{:S(2)}, u32[]{:S(2)}) collective-permute-start(bf16[1536,512]{1,0:T(8,128)(2,1)} %maximum_select_fusion.12), channel_id=1, source_target_pairs={{0,16},{8,24},{16,0},{24,8},{32,48},{40,56},{48,32},{56,40},{64,80... | collective-permute-start | bytes 4718600 | tf_op jit(solution)/shard_map/ppermute | solution.py:14
  88.8 67.0 %collective-permute-start.2 = (bf16[1536,1024]{1,0:T(8,128)(2,1)}, bf16[1536,1024]{1,0:T(8,128)(2,1)}, u32[]{:S(2)}, u32[]{:S(2)}) collective-permute-start(bf16[1536,1024]{1,0:T(8,128)(2,1)} %maximum_select_fusion.3), channel_id=1, source_target_pairs={{0,32},{8,40},{16,48},{24,56},{32,0},{40,8},{48,16},{56,24},{64,96... | collective-permute-start | bytes 9437192 | tf_op jit(solution)/shard_map/ppermute | solution.py:14
  166.0 161.7 %collective-permute-start.3 = (bf16[1536,2048]{1,0:T(8,128)(2,1)}, bf16[1536,2048]{1,0:T(8,128)(2,1)}, u32[]{:S(2)}, u32[]{:S(2)}) collective-permute-start(bf16[1536,2048]{1,0:T(8,128)(2,1)} %maximum_select_fusion.2), channel_id=1, source_target_pairs={{0,64},{8,72},{16,80},{24,88},{32,96},{40,104},{48,112},{56,120},{... | collective-permute-start | bytes 18874376 | tf_op jit(solution)/shard_map/ppermute | solution.py:14
  171.9 151.9 %all-to-all-start.1 = ((bf16[256,16,256]{0,2,1:T(8,128)(2,1)}), bf16[256,16,256]{0,2,1:T(8,128)(2,1)}, u32[]{:S(2)}, u32[]{:S(2)}) async-start(bf16[256,16,256]{0,2,1:T(8,128)(2,1)} %bitcast.8), calls=%async_computation.1 | async-start | bytes 4194304 | tf_op jit(solution)/shard_map/all_to_all | solution.py:59
  176.4 261.4 %all-gather.2.cloned.1.call-start = ((), (), s32[]{:S(2)}) async-start(), calls=%async_computation.4 | async-start | bytes 13369344 | tf_op jit(solution)/shard_map/all_gather | solution.py:68
  485.3 1.2 copy-start.1
  486.5 13.9 %copy-start.4 = (f32[256]{0:T(256)S(1)}, f32[256]{0:T(256)}, u32[]{:S(2)}) copy-start(f32[256]{0:T(256)} %param.15) | copy-start | bytes 3076
  486.5 13.9 %copy-start.5 = (f32[256]{0:T(256)S(1)}, f32[256]{0:T(256)}, u32[]{:S(2)}) copy-start(f32[256]{0:T(256)} %param.14) | copy-start | bytes 3076
Sparse Core Ops, SparseCore 0:
  340.4 97.4 all-gather.1
